TPU v7x, 32 devices: a whole 2x2x4 slice. The times are simulated.
32 devices in a mesh: row: 4 (over y, x), col: 8 (over z, core).
Axes of the slice: x: 2, y: 2, z: 4, core: 2. Of those that a mesh axis runs over, the one named last changes fastest.
Arguments:
- tokens: bfloat16 [2, 2048, 1024], P(None, ('row', 'col')), may hold values from -6 to 6
- proj_weight: bfloat16 [1024, 256], replicated, may hold values from -0.1875 to 0.1875
- gate_weight: bfloat16 [1024, 256], replicated, may hold values from -0.1875 to 0.1875
- out_weight: bfloat16 [256, 1024], replicated, may hold values from -0.375 to 0.375
Outputs:
- mixed_out: bfloat16 [2, 2048, 1024], P(None, ('col', 'row'))
All inputs are finite; a program needn't handle non-finite values.
Results may differ from a plain program's by a relative error of at most 0.02.
Values may be sent and summed in bfloat16 or wider, within the bound.
A program may use at most 64 MiB of HBM per device.

v0:
```python
import math
import jax
import jax.numpy as jnp
from jax import lax
from jax.sharding import PartitionSpec as P

GROUPS = 4
GROUP_DIM = 64


def as_sent(x):
    return jax.tree.map(lambda a: a.astype(jnp.bfloat16) if a.dtype == jnp.float32 else a, x)


def channel_tables(table_size):
    index_vec = jnp.arange(table_size, dtype=jnp.int32)
    turns_mod = index_vec[:, None] * index_vec[None, :] % table_size
    angles = 2.0 * math.pi / table_size * turns_mod.astype(jnp.float32)
    norm_scale = 1.0 / math.sqrt(table_size)
    return (jnp.cos(angles) * norm_scale, jnp.sin(angles) * norm_scale)


def channel_section(mix_input):
    seq_count, tok_rows = (mix_input.shape[0], mix_input.shape[1])
    grouped = mix_input.astype(jnp.float32).reshape(seq_count, tok_rows, GROUPS, GROUP_DIM)
    cos_table, sin_table = channel_tables(GROUP_DIM)
    real_part = jnp.einsum("stgn,nk->tsgk", grouped, cos_table, precision=lax.Precision.HIGHEST)
    imag_part = -jnp.einsum("stgn,nk->tsgk", grouped, sin_table, precision=lax.Precision.HIGHEST)
    return (real_part.reshape(tok_rows, -1), imag_part.reshape(tok_rows, -1))


def row_factor(real_part, imag_part, col_start, length_all):
    row_count, tok_rows, col_width = real_part.shape
    cos_table, sin_table = channel_tables(row_count)
    cos_table = cos_table * math.sqrt(row_count)
    sin_table = sin_table * math.sqrt(row_count)
    high = lax.Precision.HIGHEST
    first_real = jnp.einsum("ka,atm->ktm", cos_table, real_part, precision=high) + jnp.einsum(
        "ka,atm->ktm", sin_table, imag_part, precision=high
    )
    first_imag = jnp.einsum("ka,atm->ktm", cos_table, imag_part, precision=high) - jnp.einsum(
        "ka,atm->ktm", sin_table, real_part, precision=high
    )
    index_vec = jnp.arange(row_count, dtype=jnp.int32)
    position = col_start + jnp.arange(tok_rows, dtype=jnp.int32)
    turns_mod = index_vec[:, None] * position[None, :] % length_all
    angles = 2.0 * math.pi / length_all * turns_mod.astype(jnp.float32)
    twiddle_cos = jnp.cos(angles)[:, :, None]
    twiddle_sin = jnp.sin(angles)[:, :, None]
    turned_real = twiddle_cos * first_real + twiddle_sin * first_imag
    turned_imag = twiddle_cos * first_imag - twiddle_sin * first_real
    merged_real = jnp.transpose(turned_real, (1, 0, 2)).reshape(tok_rows, row_count * col_width)
    merged_imag = jnp.transpose(turned_imag, (1, 0, 2)).reshape(tok_rows, row_count * col_width)
    return (merged_real, merged_imag)


def dense_section(real_part, imag_part, length_all):
    length = real_part.shape[0]
    block_rows = min(512, length)
    block_count = length // block_rows
    points = jnp.arange(length, dtype=jnp.int32)

    def one_block(block_start):
        freq_index = block_start + jnp.arange(block_rows, dtype=jnp.int32)
        turns_mod = freq_index[:, None] * points[None, :] % length
        angles = 2.0 * math.pi / length * turns_mod.astype(jnp.float32)
        first = jnp.dot(
            jnp.cos(angles),
            real_part,
            precision=lax.Precision.HIGHEST,
            preferred_element_type=jnp.float32,
        )
        second = jnp.dot(
            jnp.sin(angles),
            imag_part,
            precision=lax.Precision.HIGHEST,
            preferred_element_type=jnp.float32,
        )
        return first + second

    starts = jnp.arange(block_count, dtype=jnp.int32) * block_rows
    spectrum = lax.map(one_block, starts).reshape(length, real_part.shape[1])
    return (spectrum * (1.0 / math.sqrt(length_all))).astype(jnp.bfloat16)


def local_order(returned, row_count):
    tok_rows = returned.shape[0]
    return returned.reshape(tok_rows, row_count, -1).reshape(tok_rows * row_count, -1)


def body(tokens, proj_weight, gate_weight, out_weight):
    seq_count, tok_rows, model_width = tokens.shape
    flattened = tokens.reshape(seq_count * tok_rows, model_width)
    hidden = jnp.dot(flattened, proj_weight, preferred_element_type=jnp.float32).astype(
        jnp.bfloat16
    )
    gate_pre = jnp.dot(flattened, gate_weight, preferred_element_type=jnp.float32)
    mix_input = (hidden.astype(jnp.float32) * jax.nn.silu(gate_pre)).astype(jnp.bfloat16)
    real_part, imag_part = channel_section(mix_input.reshape(seq_count, tok_rows, -1))
    row_count = lax.axis_size("row")
    length_all = row_count * lax.axis_size("col") * tok_rows
    col_start = lax.axis_index("col") * tok_rows
    received = (
        lax.all_to_all(as_sent(real_part[None]), "row", split_axis=2, concat_axis=0, tiled=True),
        lax.all_to_all(as_sent(imag_part[None]), "row", split_axis=2, concat_axis=0, tiled=True),
    )
    merged_real, merged_imag = row_factor(received[0], received[1], col_start, length_all)
    moved_pair = (
        lax.all_to_all(as_sent(merged_real), "col", split_axis=1, concat_axis=0, tiled=True).astype(
            merged_real.dtype
        ),
        lax.all_to_all(as_sent(merged_imag), "col", split_axis=1, concat_axis=0, tiled=True).astype(
            merged_imag.dtype
        ),
    )
    spectrum = dense_section(moved_pair[0], moved_pair[1], length_all)
    returned = lax.all_to_all(spectrum, "col", split_axis=0, concat_axis=1, tiled=True)
    mixed_cols = lax.all_to_all(
        local_order(returned, row_count), "row", split_axis=0, concat_axis=1, tiled=True
    )
    mixed = mixed_cols.reshape(tok_rows, seq_count, -1)
    result_out = jnp.einsum("tsc,cd->std", mixed, out_weight, preferred_element_type=jnp.float32)
    return result_out.astype(jnp.bfloat16)


def solution(mesh):
    in_specs = (P(None, ("row", "col"), None), P(), P(), P())
    out_specs = P(None, ("col", "row"), None)
    return jax.shard_map(body, mesh=mesh, in_specs=in_specs, out_specs=out_specs, check_vma=False)
```

profile of v0, /device:TPU:0, one launch (start us, length us, event | category | flops | bytes accessed | tf_op | source)
XLA Modules:
  0.0 73.2 jit_solution(7594770349935760409)
XLA Ops:
  0.0 1.5 %fusion.98 = f32[128,256]{1,0:T(8,128)S(1)} fusion(bf16[128,1024]{1,0:T(8,128)(2,1)} %bitcast.95, bf16[1024,256]{1,0:T(8,128)(2,1)} %param.6), kind=kOutput, calls=%fused_computation.116 | convolution fusion | flops 67108864 | bytes 917504 | tf_op jit(solution)/shard_map/dot_general | solution.py:97
  1.5 0.2 fusion.8
  1.9 0.6 convolution_convert_fusion.1
  2.4 0.2 copy.62
  2.6 0.5 broadcast.201
  3.1 1.4 %reduce.1 = bf16[512,64]{1,0:T(8,128)(2,1)S(1)} reduce(bf16[512,1,64]{2,1,0:T(2,128)(2,1)S(1)} %bitcast.89, bf16[]{:T(256)} %broadcast.201), dimensions={1}, to_apply=%bitcast.86.reduce_sub_computation | reduce | bytes 131074
  4.6 0.8 %reshape.130 = bf16[4,2,4096]{2,1,0:T(2,128)(2,1)} reshape(bf16[512,64]{1,0:T(8,128)(2,1)S(1)} %reduce.1) | data formatting | bytes 131072
  5.4 5.2 %all-to-all-start = ((bf16[4,2,4096]{2,1,0:T(2,128)(2,1)}), bf16[4,2,4096]{2,1,0:T(2,128)(2,1)S(1)}, u32[]{:S(2)}, u32[]{:S(2)}) async-start(bf16[4,2,4096]{2,1,0:T(2,128)(2,1)} %reshape.130), calls=%async_computation | async-start | bytes 131072 | tf_op jit(solution)/shard_map/all_to_all | solution.py:104
  10.6 0.6 fusion.1
  11.4 0.2 copy.61
  11.6 1.4 %reduce = bf16[512,64]{1,0:T(8,128)(2,1)S(1)} reduce(bf16[512,1,64]{2,1,0:T(2,128)(2,1)S(1)} %bitcast.90, bf16[]{:T(256)} %broadcast.201), dimensions={1}, to_apply=%bitcast.85.reduce_sub_computation | reduce | bytes 131074
  13.1 0.8 %reshape.128 = bf16[4,2,4096]{2,1,0:T(2,128)(2,1)} reshape(bf16[512,64]{1,0:T(8,128)(2,1)S(1)} %reduce) | data formatting | bytes 131072
  13.9 1.6 %all-to-all-done = bf16[4,2,4096]{2,1,0:T(2,128)(2,1)S(1)} async-done(((bf16[4,2,4096]{2,1,0:T(2,128)(2,1)}), bf16[4,2,4096]{2,1,0:T(2,128)(2,1)S(1)}, u32[]{:S(2)}, u32[]{:S(2)}) %all-to-all-start) | async-done | bytes 65568 | tf_op jit(solution)/shard_map/all_to_all | solution.py:104
  15.4 3.3 %all-to-all-start.1 = ((bf16[4,2,4096]{2,1,0:T(2,128)(2,1)}), bf16[4,2,4096]{2,1,0:T(2,128)(2,1)S(1)}, u32[]{:S(2)}, u32[]{:S(2)}) async-start(bf16[4,2,4096]{2,1,0:T(2,128)(2,1)} %reshape.128), calls=%async_computation.1 | async-start | bytes 131072 | tf_op jit(solution)/shard_map/all_to_all | solution.py:105
  19.0 0.3 fusion.24
  19.3 4.2 %all-to-all-done.1 = bf16[4,2,4096]{2,1,0:T(2,128)(2,1)S(1)} async-done(((bf16[4,2,4096]{2,1,0:T(2,128)(2,1)}), bf16[4,2,4096]{2,1,0:T(2,128)(2,1)S(1)}, u32[]{:S(2)}, u32[]{:S(2)}) %all-to-all-start.1) | async-done | bytes 65568 | tf_op jit(solution)/shard_map/all_to_all | solution.py:105
  23.8 0.3 fusion.26
  24.1 0.3 fusion.2
  24.5 0.4 subtract_convert_fusion
  25.0 0.8 %reshape.134 = bf16[8,2,2048]{2,1,0:T(2,128)(2,1)} reshape(bf16[8,64,64]{2,1,0:T(8,128)(2,1)S(1)} %bitcast.91) | data formatting | bytes 131072
  25.8 4.9 %all-to-all-start.3 = ((bf16[8,2,2048]{2,1,0:T(2,128)(2,1)}), bf16[8,2,2048]{2,1,0:T(2,128)(2,1)S(1)}, u32[]{:S(2)}, u32[]{:S(2)}) async-start(bf16[8,2,2048]{2,1,0:T(2,128)(2,1)} %reshape.134), calls=%async_computation.3 | async-start | bytes 131072 | tf_op jit(solution)/shard_map/all_to_all | solution.py:112
  30.8 0.8 %reshape.132 = bf16[8,2,2048]{2,1,0:T(2,128)(2,1)} reshape(bf16[8,64,64]{2,1,0:T(8,128)(2,1)S(1)} %bitcast.92) | data formatting | bytes 131072
  31.6 5.0 %all-to-all-done.3 = bf16[8,2,2048]{2,1,0:T(2,128)(2,1)S(1)} async-done(((bf16[8,2,2048]{2,1,0:T(2,128)(2,1)}), bf16[8,2,2048]{2,1,0:T(2,128)(2,1)S(1)}, u32[]{:S(2)}, u32[]{:S(2)}) %all-to-all-start.3) | async-done | bytes 65568 | tf_op jit(solution)/shard_map/all_to_all | solution.py:112
  36.6 3.4 %all-to-all-start.2 = ((bf16[8,2,2048]{2,1,0:T(2,128)(2,1)}), bf16[8,2,2048]{2,1,0:T(2,128)(2,1)S(1)}, u32[]{:S(2)}, u32[]{:S(2)}) async-start(bf16[8,2,2048]{2,1,0:T(2,128)(2,1)} %reshape.132), calls=%async_computation.2 | async-start | bytes 131072 | tf_op jit(solution)/shard_map/all_to_all | solution.py:109
  40.2 0.1 all_to_all.85
  40.3 5.4 %all-to-all-done.2 = bf16[8,2,2048]{2,1,0:T(2,128)(2,1)S(1)} async-done(((bf16[8,2,2048]{2,1,0:T(2,128)(2,1)}), bf16[8,2,2048]{2,1,0:T(2,128)(2,1)S(1)}, u32[]{:S(2)}, u32[]{:S(2)}) %all-to-all-start.2) | async-done | bytes 65568 | tf_op jit(solution)/shard_map/all_to_all | solution.py:109
  46.2 4.7 %fusion.13 = f32[512,64]{0,1:T(8,128)S(1)} fusion(bf16[512,64]{0,1:T(8,128)(2,1)S(1)} %all_to_all.82), kind=kOutput, calls=%fused_computation.23 | convolution fusion | flops 204996608 | bytes 196608 | tf_op jit(solution)/shard_map/while/body/eval_jaxpr/dot_general | solution.py:67
  50.9 5.1 %fusion.5 = bf16[512,64]{0,1:T(8,128)(2,1)S(1)} fusion(f32[512,64]{0,1:T(8,128)S(1)} %fusion.13, bf16[512,64]{0,1:T(8,128)(2,1)S(1)} %all_to_all.85), kind=kOutput, calls=%fused_computation.14 | convolution fusion | flops 205094912 | bytes 262144 | tf_op jit(solution)/shard_map/while/body/eval_jaxpr/dot_general | solution.py:73
  56.1 0.2 reshape.136
  56.3 8.3 %all_to_all.97 = bf16[8,2,2048]{2,1,0:T(2,128)(2,1)S(1)} all-to-all(bf16[8,2,2048]{2,1,0:T(2,128)(2,1)S(1)} %reshape.136), channel_id=1, replica_groups=mesh['row'=4,'col'=8] {'col'}, dimensions={0} | all-to-all | bytes 131072 | tf_op jit(solution)/shard_map/all_to_all | solution.py:117
  65.0 7.2 %all_to_all.98 = bf16[4,64,128]{2,1,0:T(8,128)(2,1)S(1)} all-to-all(bf16[4,64,128]{2,1,0:T(8,128)(2,1)S(1)} %all_to_all.88), channel_id=1, replica_groups=mesh['row'=4,'col'=8] {'row'}, dimensions={0} | all-to-all | bytes 131072 | tf_op jit(solution)/shard_map/all_to_all | solution.py:118
  72.3 0.9 %fusion = bf16[2,64,1024]{2,1,0:T(8,128)(2,1)} fusion(bf16[256,1024]{1,0:T(8,128)(2,1)S(1)} %copy-done, bf16[64,2,256]{2,1,0:T(2,128)(2,1)S(1)} %reshape.122), kind=kOutput, calls=%fused_computation.4 | convolution fusion | flops 67239936 | bytes 851968 | tf_op jit(solution)/shard_map/tsc,cd->std/dot_general | solution.py:122
  (32 shorter events, 2.4 us)
Async XLA Ops:
  0.0 72.3 %copy-start = (bf16[256,1024]{1,0:T(8,128)(2,1)S(1)}, bf16[256,1024]{1,0:T(8,128)(2,1)}, u32[]{:S(2)}) copy-start(bf16[256,1024]{1,0:T(8,128)(2,1)} %param.7) | copy-start | bytes 1572868
  0.0 1.5 %copy-start.2 = (bf16[1024,256]{1,0:T(8,128)(2,1)S(1)}, bf16[1024,256]{1,0:T(8,128)(2,1)}, u32[]{:S(2)}) copy-start(bf16[1024,256]{1,0:T(8,128)(2,1)} %param.5) | copy-start | bytes 1572868
  0.0 1.5 %copy-start.1 = (bf16[2,64,1024]{2,1,0:T(8,128)(2,1)S(1)}, bf16[2,64,1024]{2,1,0:T(8,128)(2,1)}, u32[]{:S(2)}) copy-start(bf16[2,64,1024]{2,1,0:T(8,128)(2,1)} %param.4) | copy-start | bytes 786436
  5.4 10.0 %all-to-all-start = ((bf16[4,2,4096]{2,1,0:T(2,128)(2,1)}), bf16[4,2,4096]{2,1,0:T(2,128)(2,1)S(1)}, u32[]{:S(2)}, u32[]{:S(2)}) async-start(bf16[4,2,4096]{2,1,0:T(2,128)(2,1)} %reshape.130), calls=%async_computation | async-start | bytes 131072 | tf_op jit(solution)/shard_map/all_to_all | solution.py:104
  15.4 8.1 %all-to-all-start.1 = ((bf16[4,2,4096]{2,1,0:T(2,128)(2,1)}), bf16[4,2,4096]{2,1,0:T(2,128)(2,1)S(1)}, u32[]{:S(2)}, u32[]{:S(2)}) async-start(bf16[4,2,4096]{2,1,0:T(2,128)(2,1)} %reshape.128), calls=%async_computation.1 | async-start | bytes 131072 | tf_op jit(solution)/shard_map/all_to_all | solution.py:105
  25.8 10.8 %all-to-all-start.3 = ((bf16[8,2,2048]{2,1,0:T(2,128)(2,1)}), bf16[8,2,2048]{2,1,0:T(2,128)(2,1)S(1)}, u32[]{:S(2)}, u32[]{:S(2)}) async-start(bf16[8,2,2048]{2,1,0:T(2,128)(2,1)} %reshape.134), calls=%async_computation.3 | async-start | bytes 131072 | tf_op jit(solution)/shard_map/all_to_all | solution.py:112
  36.6 9.2 %all-to-all-start.2 = ((bf16[8,2,2048]{2,1,0:T(2,128)(2,1)}), bf16[8,2,2048]{2,1,0:T(2,128)(2,1)S(1)}, u32[]{:S(2)}, u32[]{:S(2)}) async-start(bf16[8,2,2048]{2,1,0:T(2,128)(2,1)} %reshape.132), calls=%async_computation.2 | async-start | bytes 131072 | tf_op jit(solution)/shard_map/all_to_all | solution.py:109
where the time goes:
time: 73.9 us; the launch traced here: 73.2 us
  starting transfers between devices  16.7 us (23%)
  waiting for transfers between devices  16.2 us (22%)
  blocking collectives  15.5 us (21%)
  matrix products  14.9 us (20%)
  local copies, waits for them, and re-layouts  6.73 us (9%)
  other arithmetic  2.94 us (4%)
    all_to_all x1, blocking collectives, body(): lax.all_to_all(spectrum, 'col', split_axis=0, concat_axis=1, tiled=True)  8.3 us
    all_to_all x1, blocking collectives, body(): lax.all_to_all(local_order(returned, row_count), 'row', split_axis=0, con...  7.21 us
    all_to_all x1, waiting for transfers between devices, body(): lax.all_to_all(as_sent(merged_real), 'col', split_axis=1, concat_axis=0,...  5.44 us
    all_to_all x1, starting transfers between devices, body(): lax.all_to_all(as_sent(real_part[None]), 'row', split_axis=2, concat_axis...  5.2 us
    dot_general x1, matrix products, one_block(): jnp.dot(jnp.sin(angles), imag_part, precision=lax.Precision.HIGHEST, pref...  5.11 us
    all_to_all x1, waiting for transfers between devices, body(): lax.all_to_all(as_sent(merged_imag), 'col', split_axis=1, concat_axis=0,...  4.98 us
    all_to_all x1, starting transfers between devices, body(): lax.all_to_all(as_sent(merged_imag), 'col', split_axis=1, concat_axis=0,...  4.88 us
    dot_general x1, matrix products, one_block(): jnp.dot(jnp.cos(angles), real_part, precision=lax.Precision.HIGHEST, pref...  4.73 us
  transfers between devices with their start and end apart: 4, of which 4 were waited for; matrix products, arithmetic and copies ran while one was open for 7% of the time, Pallas kernels for 0%

commit v1 on v0

--- a/solution.py
+++ b/solution.py
@@ -109,9 +109,15 @@
         lax.all_to_all(as_sent(merged_real), "col", split_axis=1, concat_axis=0, tiled=True).astype(
             merged_real.dtype
         ),
-        lax.all_to_all(as_sent(merged_imag), "col", split_axis=1, concat_axis=0, tiled=True).astype(
-            merged_imag.dtype
-        ),
+        jnp.concatenate(
+            lax.all_to_all(
+                jnp.stack(jnp.split(as_sent(merged_imag), lax.axis_size("col"), axis=1)),
+                "col",
+                0,
+                0,
+            ),
+            axis=0,
+        ).astype(merged_imag.dtype),
     )
     spectrum = dense_section(moved_pair[0], moved_pair[1], length_all)
     returned = lax.all_to_all(spectrum, "col", split_axis=0, concat_axis=1, tiled=True)

time: 73.9 us -> 70.6 us (0.955)
  waiting for transfers between devices: 16.2 us -> 11.5 us
  blocking collectives: 15.5 us -> 17.3 us
    all_to_all x1, waiting for transfers between devices: 4.98 us -> 0.71 us  [body(): lax.all_to_all(jnp.stack(jnp.split(as_sent(merged_imag), lax.axis_size('c...]
    all_to_all x1, blocking collectives: 8.3 us -> 10 us  [body(): lax.all_to_all(spectrum, 'col', split_axis=0, concat_axis=1, tiled=True)]
    all_to_all x1, starting transfers between devices: 4.88 us -> 3.35 us  [body(): lax.all_to_all(jnp.stack(jnp.split(as_sent(merged_imag), lax.axis_size('c...]
    all_to_all x1, starting transfers between devices: 3.35 us -> 4.88 us  [body(): lax.all_to_all(as_sent(merged_real), 'col', split_axis=1, concat_axis=0,...]
    unnamed x17 -> x25, local copies, waits for them, and re-layouts: 4.56 us -> 4.86 us
  transfers between devices with their start and end apart: 4 -> 4, of which waited for: 4 -> 4; matrix products, arithmetic and copies ran while one was open for 7% -> 14% of each run, Pallas kernels for 0% -> 0%
where the time goes in v1:
time: 70.6 us; the launch traced here: 70 us
  blocking collectives  17.3 us (25%)
  starting transfers between devices  16.7 us (24%)
  matrix products  14.5 us (21%)
  waiting for transfers between devices  11.5 us (16%)
  local copies, waits for them, and re-layouts  6.73 us (10%)
  other arithmetic  2.94 us (4%)
    all_to_all x1, blocking collectives, body(): lax.all_to_all(spectrum, 'col', split_axis=0, concat_axis=1, tiled=True)  10 us
    all_to_all x1, blocking collectives, body(): lax.all_to_all(local_order(returned, row_count), 'row', split_axis=0, con...  7.21 us
    all_to_all x1, starting transfers between devices, body(): lax.all_to_all(as_sent(real_part[None]), 'row', split_axis=2, concat_axis...  5.2 us
    all_to_all x1, waiting for transfers between devices, body(): lax.all_to_all(as_sent(merged_real), 'col', split_axis=1, concat_axis=0,...  5.05 us
    all_to_all x1, starting transfers between devices, body(): lax.all_to_all(as_sent(merged_real), 'col', split_axis=1, concat_axis=0,...  4.88 us
    unnamed x25, local copies, waits for them, and re-layouts  4.86 us
    dot_general x1, matrix products, one_block(): jnp.dot(jnp.cos(angles), real_part, precision=lax.Precision.HIGHEST, pref...  4.73 us
    dot_general x1, matrix products, one_block(): jnp.dot(jnp.sin(angles), imag_part, precision=lax.Precision.HIGHEST, pref...  4.72 us
  transfers between devices with their start and end apart: 4, of which 4 were waited for; matrix products, arithmetic and copies ran while one was open for 14% of the time, Pallas kernels for 0%

profile of v1, /device:TPU:0, one launch (start us, length us, event | category | flops | bytes accessed | tf_op | source)
XLA Modules:
  0.0 70.0 jit_solution(6068337550654276730)
XLA Ops:
  0.0 1.5 %fusion.98 = f32[128,256]{1,0:T(8,128)S(1)} fusion(bf16[128,1024]{1,0:T(8,128)(2,1)} %bitcast.131, bf16[1024,256]{1,0:T(8,128)(2,1)} %param.6), kind=kOutput, calls=%fused_computation.132 | convolution fusion | flops 67108864 | bytes 917504 | tf_op jit(solution)/shard_map/dot_general | solution.py:97
  1.5 0.2 fusion.8
  1.9 0.6 convolution_convert_fusion.1
  2.4 0.2 copy.59
  2.6 0.5 broadcast.201
  3.1 1.4 %reduce.1 = bf16[512,64]{1,0:T(8,128)(2,1)S(1)} reduce(bf16[512,1,64]{2,1,0:T(2,128)(2,1)S(1)} %bitcast.118, bf16[]{:T(256)} %broadcast.201), dimensions={1}, to_apply=%bitcast.115.reduce_sub_computation | reduce | bytes 131074
  4.6 0.8 %reshape.130 = bf16[4,2,4096]{2,1,0:T(2,128)(2,1)} reshape(bf16[512,64]{1,0:T(8,128)(2,1)S(1)} %reduce.1) | data formatting | bytes 131072
  5.4 5.2 %all-to-all-start = ((bf16[4,2,4096]{2,1,0:T(2,128)(2,1)}), bf16[4,2,4096]{2,1,0:T(2,128)(2,1)S(1)}, u32[]{:S(2)}, u32[]{:S(2)}) async-start(bf16[4,2,4096]{2,1,0:T(2,128)(2,1)} %reshape.130), calls=%async_computation | async-start | bytes 131072 | tf_op jit(solution)/shard_map/all_to_all | solution.py:104
  10.6 0.6 fusion.1
  11.4 0.2 copy.58
  11.6 1.4 %reduce = bf16[512,64]{1,0:T(8,128)(2,1)S(1)} reduce(bf16[512,1,64]{2,1,0:T(2,128)(2,1)S(1)} %bitcast.119, bf16[]{:T(256)} %broadcast.201), dimensions={1}, to_apply=%bitcast.114.reduce_sub_computation | reduce | bytes 131074
  13.1 0.8 %reshape.128 = bf16[4,2,4096]{2,1,0:T(2,128)(2,1)} reshape(bf16[512,64]{1,0:T(8,128)(2,1)S(1)} %reduce) | data formatting | bytes 131072
  13.9 1.6 %all-to-all-done = bf16[4,2,4096]{2,1,0:T(2,128)(2,1)S(1)} async-done(((bf16[4,2,4096]{2,1,0:T(2,128)(2,1)}), bf16[4,2,4096]{2,1,0:T(2,128)(2,1)S(1)}, u32[]{:S(2)}, u32[]{:S(2)}) %all-to-all-start) | async-done | bytes 65568 | tf_op jit(solution)/shard_map/all_to_all | solution.py:104
  15.4 3.3 %all-to-all-start.1 = ((bf16[4,2,4096]{2,1,0:T(2,128)(2,1)}), bf16[4,2,4096]{2,1,0:T(2,128)(2,1)S(1)}, u32[]{:S(2)}, u32[]{:S(2)}) async-start(bf16[4,2,4096]{2,1,0:T(2,128)(2,1)} %reshape.128), calls=%async_computation.1 | async-start | bytes 131072 | tf_op jit(solution)/shard_map/all_to_all | solution.py:105
  19.0 0.3 fusion.24
  19.3 4.2 %all-to-all-done.1 = bf16[4,2,4096]{2,1,0:T(2,128)(2,1)S(1)} async-done(((bf16[4,2,4096]{2,1,0:T(2,128)(2,1)}), bf16[4,2,4096]{2,1,0:T(2,128)(2,1)S(1)}, u32[]{:S(2)}, u32[]{:S(2)}) %all-to-all-start.1) | async-done | bytes 65568 | tf_op jit(solution)/shard_map/all_to_all | solution.py:105
  23.8 0.3 fusion.26
  24.1 0.3 fusion.2
  24.5 0.4 subtract_convert_fusion
  25.3 0.8 %reshape.132 = bf16[8,2,2048]{2,1,0:T(2,128)(2,1)} reshape(bf16[8,64,64]{2,1,0:T(8,128)(2,1)S(1)} %bitcast.128) | data formatting | bytes 131072
  26.1 4.9 %all-to-all-start.2 = ((bf16[8,2,2048]{2,1,0:T(2,128)(2,1)}), bf16[8,2,2048]{2,1,0:T(2,128)(2,1)S(1)}, u32[]{:S(2)}, u32[]{:S(2)}) async-start(bf16[8,2,2048]{2,1,0:T(2,128)(2,1)} %reshape.132), calls=%async_computation.2 | async-start | bytes 131072 | tf_op jit(solution)/shard_map/all_to_all | solution.py:109
  31.1 0.8 %reshape.134 = bf16[8,2,2048]{2,1,0:T(2,128)(2,1)} reshape(bf16[8,64,64]{2,1,0:T(8,128)(2,1)S(1)} %constant_dynamic-update-slice_fusion) | data formatting | bytes 131072
  31.8 5.1 %all-to-all-done.2 = bf16[8,2,2048]{2,1,0:T(2,128)(2,1)S(1)} async-done(((bf16[8,2,2048]{2,1,0:T(2,128)(2,1)}), bf16[8,2,2048]{2,1,0:T(2,128)(2,1)S(1)}, u32[]{:S(2)}, u32[]{:S(2)}) %all-to-all-start.2) | async-done | bytes 65568 | tf_op jit(solution)/shard_map/all_to_all | solution.py:109
  36.9 3.3 %all-to-all-start.3 = ((bf16[8,2,2048]{2,1,0:T(2,128)(2,1)}), bf16[8,2,2048]{2,1,0:T(2,128)(2,1)S(1)}, u32[]{:S(2)}, u32[]{:S(2)}) async-start(bf16[8,2,2048]{2,1,0:T(2,128)(2,1)} %reshape.134), calls=%async_computation.3 | async-start | bytes 131072 | tf_op jit(solution)/shard_map/all_to_all | solution.py:113
  40.5 0.1 all_to_all.73
  40.7 4.7 %fusion.13 = f32[512,64]{0,1:T(8,128)S(1)} fusion(bf16[512,64]{0,1:T(8,128)(2,1)S(1)} %all_to_all.73), kind=kOutput, calls=%fused_computation.23 | convolution fusion | flops 204996608 | bytes 196608 | tf_op jit(solution)/shard_map/while/body/eval_jaxpr/dot_general | solution.py:67
  45.4 0.7 %all-to-all-done.3 = bf16[8,2,2048]{2,1,0:T(2,128)(2,1)S(1)} async-done(((bf16[8,2,2048]{2,1,0:T(2,128)(2,1)}), bf16[8,2,2048]{2,1,0:T(2,128)(2,1)S(1)}, u32[]{:S(2)}, u32[]{:S(2)}) %all-to-all-start.3) | async-done | bytes 65568 | tf_op jit(solution)/shard_map/all_to_all | solution.py:113
  46.2 4.7 %fusion.5 = bf16[512,64]{0,1:T(8,128)(2,1)S(1)} fusion(f32[512,64]{0,1:T(8,128)S(1)} %fusion.13, bf16[512,64]{1,0:T(8,128)(2,1)S(1)} %bitcast.136), kind=kOutput, calls=%fused_computation.14 | convolution fusion | flops 205094912 | bytes 262144 | tf_op jit(solution)/shard_map/while/body/eval_jaxpr/dot_general | solution.py:73
  51.1 0.2 reshape.136
  51.3 10.0 %all_to_all.86 = bf16[8,2,2048]{2,1,0:T(2,128)(2,1)S(1)} all-to-all(bf16[8,2,2048]{2,1,0:T(2,128)(2,1)S(1)} %reshape.136), channel_id=1, replica_groups=mesh['row'=4,'col'=8] {'col'}, dimensions={0} | all-to-all | bytes 131072 | tf_op jit(solution)/shard_map/all_to_all | solution.py:123
  61.7 7.2 %all_to_all.87 = bf16[4,64,128]{2,1,0:T(8,128)(2,1)S(1)} all-to-all(bf16[4,64,128]{2,1,0:T(8,128)(2,1)S(1)} %all_to_all.77), channel_id=1, replica_groups=mesh['row'=4,'col'=8] {'row'}, dimensions={0} | all-to-all | bytes 131072 | tf_op jit(solution)/shard_map/all_to_all | solution.py:124
  69.0 0.9 %fusion = bf16[2,64,1024]{2,1,0:T(8,128)(2,1)} fusion(bf16[256,1024]{1,0:T(8,128)(2,1)S(1)} %copy-done, bf16[64,2,256]{2,1,0:T(2,128)(2,1)S(1)} %reshape.122), kind=kOutput, calls=%fused_computation.4 | convolution fusion | flops 67239936 | bytes 851968 | tf_op jit(solution)/shard_map/tsc,cd->std/dot_general | solution.py:128
  (37 shorter events, 2.4 us)
Async XLA Ops:
  0.0 69.0 %copy-start = (bf16[256,1024]{1,0:T(8,128)(2,1)S(1)}, bf16[256,1024]{1,0:T(8,128)(2,1)}, u32[]{:S(2)}) copy-start(bf16[256,1024]{1,0:T(8,128)(2,1)} %param.7) | copy-start | bytes 1572868
  0.0 1.5 %copy-start.2 = (bf16[1024,256]{1,0:T(8,128)(2,1)S(1)}, bf16[1024,256]{1,0:T(8,128)(2,1)}, u32[]{:S(2)}) copy-start(bf16[1024,256]{1,0:T(8,128)(2,1)} %param.5) | copy-start | bytes 1572868
  0.0 1.5 %copy-start.1 = (bf16[2,64,1024]{2,1,0:T(8,128)(2,1)S(1)}, bf16[2,64,1024]{2,1,0:T(8,128)(2,1)}, u32[]{:S(2)}) copy-start(bf16[2,64,1024]{2,1,0:T(8,128)(2,1)} %param.4) | copy-start | bytes 786436
  5.4 10.0 %all-to-all-start = ((bf16[4,2,4096]{2,1,0:T(2,128)(2,1)}), bf16[4,2,4096]{2,1,0:T(2,128)(2,1)S(1)}, u32[]{:S(2)}, u32[]{:S(2)}) async-start(bf16[4,2,4096]{2,1,0:T(2,128)(2,1)} %reshape.130), calls=%async_computation | async-start | bytes 131072 | tf_op jit(solution)/shard_map/all_to_all | solution.py:104
  15.4 8.1 %all-to-all-start.1 = ((bf16[4,2,4096]{2,1,0:T(2,128)(2,1)}), bf16[4,2,4096]{2,1,0:T(2,128)(2,1)S(1)}, u32[]{:S(2)}, u32[]{:S(2)}) async-start(bf16[4,2,4096]{2,1,0:T(2,128)(2,1)} %reshape.128), calls=%async_computation.1 | async-start | bytes 131072 | tf_op jit(solution)/shard_map/all_to_all | solution.py:105
  26.1 10.8 %all-to-all-start.2 = ((bf16[8,2,2048]{2,1,0:T(2,128)(2,1)}), bf16[8,2,2048]{2,1,0:T(2,128)(2,1)S(1)}, u32[]{:S(2)}, u32[]{:S(2)}) async-start(bf16[8,2,2048]{2,1,0:T(2,128)(2,1)} %reshape.132), calls=%async_computation.2 | async-start | bytes 131072 | tf_op jit(solution)/shard_map/all_to_all | solution.py:109
  36.9 9.2 %all-to-all-start.3 = ((bf16[8,2,2048]{2,1,0:T(2,128)(2,1)}), bf16[8,2,2048]{2,1,0:T(2,128)(2,1)S(1)}, u32[]{:S(2)}, u32[]{:S(2)}) async-start(bf16[8,2,2048]{2,1,0:T(2,128)(2,1)} %reshape.134), calls=%async_computation.3 | async-start | bytes 131072 | tf_op jit(solution)/shard_map/all_to_all | solution.py:113
